TPU v7x, 256 devices: a whole 4x4x8 slice. The times are simulated.
256 devices in a mesh: ep: 64 (over z, x, core), tp: 4 (over y).
Axes of the slice: x: 4, y: 4, z: 8, core: 2. Of those that a mesh axis runs over, the one named last changes fastest.
Arguments:
- tokens: bfloat16 [65536, 2048], P(('ep', 'tp')), may hold values from -6 to 6
- norm_gain: bfloat16 [2048], replicated, may hold values from 0.099609375 to 1.8984375
- expert_ids: int32 [65536, 2], P(('ep', 'tp')), may hold values from 0 to 63, all different within a row; in each aligned block of 256 rows (0 to 255, 256 to 511, ...) at most 16 rows name the same one
- group_weight: float32 [65536], P(('ep', 'tp')), may hold values from 0.25 to 1
- expert_logit: float32 [65536, 2], P(('ep', 'tp')), may hold values from -4 to 4
- w_gate: bfloat16 [64, 2048, 1024], P('ep', None, 'tp'), may hold values from -0.125 to 0.125
- w_up: bfloat16 [64, 2048, 1024], P('ep', None, 'tp'), may hold values from -0.125 to 0.125
- w_down: bfloat16 [64, 1024, 2048], P('ep', 'tp')
- final_gain: bfloat16 [2048], P('tp'), may hold values from 0.099609375 to 1.8984375
Outputs:
- normed_out: bfloat16 [65536, 2048], P('ep', 'tp')
Inputs may be any that keep to these rules, and one draw needn't show every extreme that they name: `expert_ids`: the 2 experts of a token differ. Among the rows of one device (aligned blocks of 256 tokens) no expert is named more than 16 times, a bound that some block reaches.
All inputs are finite; a program needn't handle non-finite values.
Results may differ from a plain program's by a relative error of at most 0.0058.
Values may be sent and summed in bfloat16 or wider, within the bound.
A program may use at most 128 MiB of HBM per device.

v0:
```python
import jax
import jax.numpy as jnp
from jax import lax
from jax.sharding import PartitionSpec as P

D = 2048
CAP = 16
EPS = 1e-06


def local(
    tokens, norm_gain, expert_ids, group_weight, expert_logit, w_gate, w_up, w_down, final_gain
):
    rows, width = tokens.shape
    experts = lax.axis_size("ep")
    slots = experts * CAP
    down_whole = lax.all_gather(w_down, "tp", axis=1, tiled=True)[0]
    both = lax.all_gather(jnp.concatenate((w_gate, w_up), axis=0), "tp", axis=2, tiled=True)
    tokens_f = tokens.astype(jnp.float32)
    inverse_in = lax.rsqrt(jnp.mean(tokens_f * tokens_f, axis=-1, keepdims=True) + EPS)
    normed_in = (tokens_f * inverse_in * norm_gain.astype(jnp.float32)).astype(jnp.bfloat16)
    lane = jnp.arange(experts, dtype=jnp.int32)[None, :]
    first = expert_ids[:, 0:1] == lane
    second = expert_ids[:, 1:2] == lane
    named = (first | second).astype(jnp.bfloat16)
    order = jnp.arange(rows, dtype=jnp.int32)
    earlier = (order[:, None] > order[None, :]).astype(jnp.bfloat16)
    before = jnp.dot(earlier, named, preferred_element_type=jnp.float32)
    rank0 = jnp.sum(jnp.where(first, before, 0.0), axis=1).astype(jnp.int32)
    rank1 = jnp.sum(jnp.where(second, before, 0.0), axis=1).astype(jnp.int32)
    at0 = expert_ids[:, 0] * CAP + rank0
    at1 = expert_ids[:, 1] * CAP + rank1
    slot = jnp.arange(slots, dtype=jnp.int32)
    pick = ((slot[:, None] == at0[None, :]) | (slot[:, None] == at1[None, :])).astype(jnp.bfloat16)
    outgoing = jnp.dot(pick, normed_in, preferred_element_type=jnp.float32).astype(jnp.bfloat16)
    incoming = lax.all_to_all(
        outgoing.reshape(experts, CAP, width), "ep", split_axis=0, concat_axis=0, tiled=True
    )
    routed = incoming.reshape(slots, width)
    gate_full = jnp.dot(routed, both[0], preferred_element_type=jnp.float32)
    up_full = jnp.dot(routed, both[1], preferred_element_type=jnp.float32)
    hidden = (jax.nn.silu(gate_full) * up_full).astype(jnp.bfloat16)
    product = jnp.dot(hidden, down_whole, preferred_element_type=jnp.float32).astype(jnp.bfloat16)
    arrived = lax.all_to_all(
        product.reshape(experts, CAP, width), "ep", split_axis=0, concat_axis=0, tiled=True
    ).reshape(slots, width)
    share = jnp.exp(expert_logit)
    weight = group_weight[:, None] * (share / jnp.sum(share, axis=-1, keepdims=True))
    spread = jnp.where(slot[None, :] == at0[:, None], weight[:, 0:1], 0.0) + jnp.where(
        slot[None, :] == at1[:, None], weight[:, 1:2], 0.0
    )
    high = spread.astype(jnp.bfloat16)
    low = (spread - high.astype(jnp.float32)).astype(jnp.bfloat16)
    mixed = jnp.dot(high, arrived, preferred_element_type=jnp.float32) + jnp.dot(
        low, arrived, preferred_element_type=jnp.float32
    )
    residual = (tokens_f + mixed).astype(jnp.bfloat16)
    pieces = residual.reshape(rows, 4, width // 4).transpose(1, 0, 2)
    sliced = lax.all_to_all(pieces, "tp", split_axis=0, concat_axis=0, tiled=True)
    sliced = sliced.reshape(4 * rows, width // 4).astype(jnp.float32)
    squares = lax.all_gather(jnp.sum(sliced * sliced, axis=-1), "tp", axis=0).sum(axis=0)
    inverse_out = lax.rsqrt(squares / D + EPS)
    return (sliced * inverse_out[:, None] * final_gain.astype(jnp.float32)).astype(jnp.bfloat16)


def solution(mesh):
    placed = (
        P(("ep", "tp"), None),
        P(),
        P(("ep", "tp"), None),
        P(("ep", "tp")),
        P(("ep", "tp"), None),
        P("ep", None, "tp"),
        P("ep", None, "tp"),
        P("ep", "tp", None),
        P("tp"),
    )
    return jax.shard_map(
        local, mesh=mesh, in_specs=placed, out_specs=P("ep", "tp"), check_vma=False
    )
```

profile of v0, /device:TPU:38, one launch (start us, length us, event | category | flops | bytes accessed | tf_op | source)
XLA Modules:
  0.0 317.0 jit_solution(2494651620982889680)
XLA Ops:
  6.5 0.0 all-gather.4.cloned.1.call-start
  6.5 3.1 pad_maximum_fusion
  9.7 0.0 all-gather.4.cloned.1.call-update
  9.7 0.0 copy-done.3
  9.7 0.0 copy-done.2
  9.7 0.2 select_reduce_fusion.1
  10.0 0.0 copy-done
  10.0 0.3 fusion.8
  10.3 3.3 %convolution_convert_fusion = bf16[1024,2048]{1,0:T(8,128)(2,1)} fusion(bf16[256,2048]{1,0:T(8,128)(2,1)S(1)} %copy-done, f32[2048]{0:T(1024)S(1)} %convert_element_type.88, f32[256]{0:T(256)S(1)} %add_rsqrt_fusion.1, s32[256]{0:T(256)S(1)} %get-tuple-element.13, s32[256]{0:T(256)S(1)} %get-tuple-element.14), kind=kOutput, calls=%fused_computation.7 | convolution fusion | flops 1078722560 | bytes 5254144 | tf_op jit(solution)/shard_map/dot_general | solution.py:35
  13.6 11.7 %all-to-all-start = ((bf16[64,16,2048]{2,1,0:T(8,128)(2,1)}), bf16[64,16,2048]{2,1,0:T(8,128)(2,1)}, u32[]{:S(2)}, u32[]{:S(2)}) async-start(bf16[64,16,2048]{2,1,0:T(8,128)(2,1)} %bitcast.43), calls=%async_computation | async-start | bytes 8388608 | tf_op jit(solution)/shard_map/all_to_all | solution.py:36
  25.3 0.0 all-gather.6.cloned.1.call-start
  25.4 0.7 all-gather.6.cloned.1.call-update
  26.1 94.5 %all-to-all-done = bf16[64,16,2048]{2,1,0:T(8,128)(2,1)} async-done(((bf16[64,16,2048]{2,1,0:T(8,128)(2,1)}), bf16[64,16,2048]{2,1,0:T(8,128)(2,1)}, u32[]{:S(2)}, u32[]{:S(2)}) %all-to-all-start) | async-done | bytes 4194336 | tf_op jit(solution)/shard_map/all_to_all | solution.py:36
  120.6 7.6 %fusion = f32[1024,1024]{1,0:T(8,128)S(1)} fusion(bf16[1024,2048]{1,0:T(8,128)(2,1)} %bitcast.9, bf16[2,2048,1024]{2,1,0:T(8,128)(2,1)} %all-gather.4.cloned.1.call-done), kind=kOutput, calls=%fused_computation.1 | convolution fusion | flops 4294967296 | bytes 12582912 | tf_op jit(solution)/shard_map/dot_general | solution.py:41
  128.3 0.0 copy-done.6
  128.3 7.6 %multiply_convert_fusion = bf16[1024,1024]{1,0:T(8,128)(2,1)S(1)} fusion(f32[1024,1024]{1,0:T(8,128)S(1)} %fusion, bf16[1024,2048]{1,0:T(8,128)(2,1)} %bitcast.9, bf16[2,2048,1024]{2,1,0:T(8,128)(2,1)S(1)} %copy-done.6), kind=kOutput, calls=%fused_computation.6 | convolution fusion | flops 4301258752 | bytes 14680064 | tf_op jit(solution)/shard_map/dot_general | solution.py:40
  135.9 18.9 %all-gather.6.cloned.1.call-done = bf16[1,1024,2048]{2,1,0:T(8,128)(2,1)} async-done(((bf16[1,256,2048]{2,1,0:T(8,128)(2,1)}), bf16[1,1024,2048]{2,1,0:T(8,128)(2,1)}) %all-gather.6.cloned.1.call-update) | async-done | bytes 4194320 | tf_op jit(solution)/shard_map/all_gather | solution.py:17
  154.8 8.2 %fusion.4 = bf16[1024,2048]{1,0:T(8,128)(2,1)} fusion(bf16[1024,1024]{1,0:T(8,128)(2,1)S(1)} %multiply_convert_fusion, bf16[1,1024,2048]{2,1,0:T(8,128)(2,1)} %all-gather.6.cloned.1.call-done), kind=kOutput, calls=%fused_computation.8 | convolution fusion | flops 4297064448 | bytes 10485760 | tf_op jit(solution)/shard_map/dot_general | solution.py:43
  163.0 10.8 %all-to-all-start.1 = ((bf16[64,16,2048]{2,1,0:T(8,128)(2,1)}), bf16[64,16,2048]{2,1,0:T(8,128)(2,1)}, u32[]{:S(2)}, u32[]{:S(2)}) async-start(bf16[64,16,2048]{2,1,0:T(8,128)(2,1)} %bitcast.44), calls=%async_computation.1 | async-start | bytes 8388608 | tf_op jit(solution)/shard_map/all_to_all | solution.py:44
  173.8 0.0 copy-done.1
  173.8 0.0 copy-done.5
  173.9 95.1 %all-to-all-done.1 = bf16[64,16,2048]{2,1,0:T(8,128)(2,1)} async-done(((bf16[64,16,2048]{2,1,0:T(8,128)(2,1)}), bf16[64,16,2048]{2,1,0:T(8,128)(2,1)}, u32[]{:S(2)}, u32[]{:S(2)}) %all-to-all-start.1) | async-done | bytes 4194336 | tf_op jit(solution)/shard_map/all_to_all | solution.py:44
  269.0 3.6 %fusion.27 = f32[256,2048]{1,0:T(8,128)S(1)} fusion(bf16[1024,2048]{1,0:T(8,128)(2,1)} %bitcast.14, f32[256]{0:T(256)S(1)} %bitcast.54, s32[256]{0:T(256)S(1)} %bitcast.58, f32[256]{0:T(256)S(1)} %bitcast.52, s32[256]{0:T(256)S(1)} %bitcast.56), kind=kOutput, calls=%fused_computation.40 | convolution fusion | flops 1075314688 | bytes 6295552 | tf_op jit(solution)/shard_map/dot_general | solution.py:54
  272.7 3.7 %fusion.7 = bf16[256,2048]{1,0:T(8,128)(2,1)S(1)} fusion(f32[256,2048]{1,0:T(8,128)S(1)} %fusion.27, bf16[1024,2048]{1,0:T(8,128)(2,1)} %bitcast.14, bf16[256,2048]{1,0:T(8,128)(2,1)S(1)} %copy-done, f32[256]{0:T(256)S(1)} %bitcast.55, s32[256]{0:T(256)S(1)} %bitcast.59, f32[256]{0:T(256)S(1)} %bitcast.53, s32[256]{0:T(256)S(1)} %bitcast.57), kind=kOutput, calls=%fused_computation.13 | convolution fusion | flops 1078198272 | bytes 8392704 | tf_op jit(solution)/shard_map/dot_general | solution.py:54
  276.4 0.0 copy-start.4
  276.4 1.1 copy.19
  277.5 3.5 %all-to-all-start.2 = ((bf16[4,256,512]{2,1,0:T(8,128)(2,1)}), bf16[4,256,512]{2,1,0:T(8,128)(2,1)S(1)}, u32[]{:S(2)}, u32[]{:S(2)}) async-start(bf16[4,256,512]{2,1,0:T(8,128)(2,1)} %bitcast.42), calls=%async_computation.2 | async-start | bytes 2097152 | tf_op jit(solution)/shard_map/all_to_all | solution.py:59
  281.0 0.0 copy-done.4
  281.0 15.5 %all-to-all-done.2 = bf16[4,256,512]{2,1,0:T(8,128)(2,1)S(1)} async-done(((bf16[4,256,512]{2,1,0:T(8,128)(2,1)}), bf16[4,256,512]{2,1,0:T(8,128)(2,1)S(1)}, u32[]{:S(2)}, u32[]{:S(2)}) %all-to-all-start.2) | async-done | bytes 1048608 | tf_op jit(solution)/shard_map/all_to_all | solution.py:59
  296.5 0.3 multiply_reduce_fusion
  296.8 12.0 %all-gather = f32[4,1,1024]{2,1,0:T(1,128)S(1)} all-gather(f32[1,1,1024]{2,1,0:T(1,128)S(1)} %reshape.77), channel_id=1, replica_groups=mesh['ep'=64,'tp'=4] {'tp'}, dimensions={0}, use_global_device_ids=true | all-gather | bytes 20480 | tf_op jit(solution)/shard_map/all_gather | solution.py:61
  308.8 1.3 fusion.12
  (21 shorter events, 0.1 us)
Async XLA Ops:
  6.5 3.2 copy-start.3
  6.5 3.2 %copy-start.2 = (s32[256,2]{0,1:T(2,128)S(1)}, s32[256,2]{0,1:T(2,128)}, u32[]{:S(2)}) copy-start(s32[256,2]{0,1:T(2,128)} %param.11) | copy-start | bytes 6148
  6.5 3.4 %copy-start = (bf16[256,2048]{1,0:T(8,128)(2,1)S(1)}, bf16[256,2048]{1,0:T(8,128)(2,1)}, u32[]{:S(2)}) copy-start(bf16[256,2048]{1,0:T(8,128)(2,1)} %param.9) | copy-start | bytes 3145732
  6.5 114.1 %all-gather.4.cloned.1.call-start = ((), (), s32[]{:S(2)}) async-start(), calls=%async_computation.3 | async-start | bytes 10485760 | tf_op jit(solution)/shard_map/all_gather | solution.py:18
  13.6 107.0 %all-to-all-start = ((bf16[64,16,2048]{2,1,0:T(8,128)(2,1)}), bf16[64,16,2048]{2,1,0:T(8,128)(2,1)}, u32[]{:S(2)}, u32[]{:S(2)}) async-start(bf16[64,16,2048]{2,1,0:T(8,128)(2,1)} %bitcast.43), calls=%async_computation | async-start | bytes 8388608 | tf_op jit(solution)/shard_map/all_to_all | solution.py:36
  25.3 129.5 %all-gather.6.cloned.1.call-start = ((), (), s32[]{:S(2)}) async-start(), calls=%async_computation.4 | async-start | bytes 5242880 | tf_op jit(solution)/shard_map/all_gather | solution.py:17
  120.6 7.7 %copy-start.6 = (bf16[2,2048,1024]{2,1,0:T(8,128)(2,1)S(1)}, bf16[2,2048,1024]{2,1,0:T(8,128)(2,1)}, u32[]{:S(2)}) copy-start(bf16[2,2048,1024]{2,1,0:T(8,128)(2,1)} %all-gather.4.cloned.1.call-done) | copy-start | bytes 25165828
  163.0 10.8 %copy-start.1 = (f32[256,2]{0,1:T(2,128)S(1)}, f32[256,2]{0,1:T(2,128)}, u32[]{:S(2)}) copy-start(f32[256,2]{0,1:T(2,128)} %param.13) | copy-start | bytes 6148
  163.0 10.8 %copy-start.5 = (f32[256]{0:T(256)S(1)}, f32[256]{0:T(256)}, u32[]{:S(2)}) copy-start(f32[256]{0:T(256)} %param.12) | copy-start | bytes 3076
  163.0 106.0 %all-to-all-start.1 = ((bf16[64,16,2048]{2,1,0:T(8,128)(2,1)}), bf16[64,16,2048]{2,1,0:T(8,128)(2,1)}, u32[]{:S(2)}, u32[]{:S(2)}) async-start(bf16[64,16,2048]{2,1,0:T(8,128)(2,1)} %bitcast.44), calls=%async_computation.1 | async-start | bytes 8388608 | tf_op jit(solution)/shard_map/all_to_all | solution.py:44
  276.4 4.6 %copy-start.4 = (bf16[512]{0:T(512)(128)(2,1)S(1)}, bf16[512]{0:T(512)(128)(2,1)}, u32[]{:S(2)}) copy-start(bf16[512]{0:T(512)(128)(2,1)} %param.17) | copy-start | bytes 3076
  277.5 19.0 %all-to-all-start.2 = ((bf16[4,256,512]{2,1,0:T(8,128)(2,1)}), bf16[4,256,512]{2,1,0:T(8,128)(2,1)S(1)}, u32[]{:S(2)}, u32[]{:S(2)}) async-start(bf16[4,256,512]{2,1,0:T(8,128)(2,1)} %bitcast.42), calls=%async_computation.2 | async-start | bytes 2097152 | tf_op jit(solution)/shard_map/all_to_all | solution.py:59
Sparse Core Ops, SparseCore 0:
  9.8 91.9 all-gather.3
  103.6 51.0 all-gather.5
where the time goes:
time: 317 us
  waiting for transfers between devices  225 us (71%)
  matrix products  34.3 us (11%)
  starting transfers between devices  26 us (8%)
  between operations  13.6 us (4%)
  blocking collectives  12 us (4%)
  other arithmetic  5.08 us (2%)
    all_to_all x1, waiting for transfers between devices, local(): lax.all_to_all(product.reshape(experts, CAP, width), 'ep', split_axis=0,...  95.1 us
    all_to_all x1, waiting for transfers between devices, local(): lax.all_to_all(outgoing.reshape(experts, CAP, width), 'ep', split_axis=0,...  94.5 us
    all_gather x1, waiting for transfers between devices, local(): down_whole = lax.all_gather(w_down, 'tp', axis=1, tiled=True)[0]  18.9 us
    all_to_all x1, waiting for transfers between devices, local(): lax.all_to_all(pieces, 'tp', split_axis=0, concat_axis=0, tiled=True)  15.5 us
    all_gather x1, blocking collectives, local(): lax.all_gather(jnp.sum(sliced * sliced, axis=-1), 'tp', axis=0).sum(axis=0)  12 us
    all_to_all x1, starting transfers between devices, local(): lax.all_to_all(outgoing.reshape(experts, CAP, width), 'ep', split_axis=0,...  11.7 us
    all_to_all x1, starting transfers between devices, local(): lax.all_to_all(product.reshape(experts, CAP, width), 'ep', split_axis=0,...  10.8 us
    dot_general x1, matrix products, local(): jnp.dot(hidden, down_whole, preferred_element_type=jnp.float32)  8.2 us
  transfers between devices with their start and end apart: 5, of which 4 were waited for; matrix products, arithmetic and copies ran while one was open for 6% of the time, Pallas kernels for 0%

commit v1 on v0

--- a/solution.py
+++ b/solution.py
@@ -8,13 +8,23 @@
 EPS = 1e-06
 
 
+def ring_gather(x, axis, dim):
+    ways, here, step = (lax.axis_size(axis), lax.axis_index(axis), x.shape[dim])
+    lengths = [n * ways if d == dim else n for d, n in enumerate(x.shape)]
+    full = lax.dynamic_update_slice_in_dim(jnp.zeros(lengths, x.dtype), x, here * step, axis=dim)
+    for far in range(1, ways):
+        x = lax.ppermute(x, axis, [(d, (d + 1) % ways) for d in range(ways)])
+        full = lax.dynamic_update_slice_in_dim(full, x, (here - far) % ways * step, axis=dim)
+    return full
+
+
 def local(
     tokens, norm_gain, expert_ids, group_weight, expert_logit, w_gate, w_up, w_down, final_gain
 ):
     rows, width = tokens.shape
     experts = lax.axis_size("ep")
     slots = experts * CAP
-    down_whole = lax.all_gather(w_down, "tp", axis=1, tiled=True)[0]
+    down_whole = ring_gather(w_down, "tp", 1)[0]
     both = lax.all_gather(jnp.concatenate((w_gate, w_up), axis=0), "tp", axis=2, tiled=True)
     tokens_f = tokens.astype(jnp.float32)
     inverse_in = lax.rsqrt(jnp.mean(tokens_f * tokens_f, axis=-1, keepdims=True) + EPS)

time: 317 us -> 349 us (1.10)
  waiting for transfers between devices: 225 us -> 243 us
  local copies, waits for them, and re-layouts: 1.12 us -> 10.4 us
    ppermute x0 -> x3, waiting for transfers between devices: none -> 133 us  [ring_gather(): x = lax.ppermute(x, axis, [(d, (d + 1) % ways) for d in range(ways)])]
    all_to_all x1, waiting for transfers between devices: 94.5 us -> 0.01 us  [local(): lax.all_to_all(outgoing.reshape(experts, CAP, width), 'ep', split_axis=0,...]
    all_gather x1 -> x0, waiting for transfers between devices: 18.9 us -> none  [local(): down_whole = lax.all_gather(w_down, 'tp', axis=1, tiled=True)[0]]
    dot_general x1 -> x0, matrix products: 7.58 us -> none  [local(): gate_full = jnp.dot(routed, both[0], preferred_element_type=jnp.float32)]
    dot_general x1, matrix products: 8.2 us -> 15.4 us  [local(): jnp.dot(hidden, down_whole, preferred_element_type=jnp.float32)]
    dynamic_update_slice x0 -> x4, local copies, waits for them, and re-layouts: none -> 6.8 us  [the longest x3 5.76 us: ring_gather(): lax.dynamic_update_slice_in_dim(full, x, (here - far) % ways * step, axis...]
  transfers between devices with their start and end apart: 5 -> 7, of which waited for: 4 -> 5; matrix products, arithmetic and copies ran while one was open for 6% -> 4% of each run, Pallas kernels for 0% -> 0%
where the time goes in v1:
time: 349 us
  waiting for transfers between devices  243 us (70%)
  matrix products  36.2 us (10%)
  starting transfers between devices  28.7 us (8%)
  between operations  13.6 us (4%)
  blocking collectives  12 us (3%)
  local copies, waits for them, and re-layouts  10.4 us (3%)
  other arithmetic  5.12 us (1%)
    ppermute x3, waiting for transfers between devices, ring_gather(): x = lax.ppermute(x, axis, [(d, (d + 1) % ways) for d in range(ways)])  133 us
    all_to_all x1, waiting for transfers between devices, local(): lax.all_to_all(product.reshape(experts, CAP, width), 'ep', split_axis=0,...  95.2 us
    dot_general x1, matrix products, local(): jnp.dot(hidden, down_whole, preferred_element_type=jnp.float32)  15.4 us
    all_to_all x1, waiting for transfers between devices, local(): lax.all_to_all(pieces, 'tp', split_axis=0, concat_axis=0, tiled=True)  15.2 us
    all_gather x1, blocking collectives, local(): lax.all_gather(jnp.sum(sliced * sliced, axis=-1), 'tp', axis=0).sum(axis=0)  12 us
    all_to_all x1, starting transfers between devices, local(): lax.all_to_all(outgoing.reshape(experts, CAP, width), 'ep', split_axis=0,...  11.8 us
    all_to_all x1, starting transfers between devices, local(): lax.all_to_all(product.reshape(experts, CAP, width), 'ep', split_axis=0,...  10.8 us
    dot_general x1, matrix products, local(): up_full = jnp.dot(routed, both[1], preferred_element_type=jnp.float32)  9.89 us
  transfers between devices with their start and end apart: 7, of which 5 were waited for; matrix products, arithmetic and copies ran while one was open for 4% of the time, Pallas kernels for 0%

profile of v1, /device:TPU:38, one launch (start us, length us, event | category | flops | bytes accessed | tf_op | source)
XLA Modules:
  0.0 349.0 jit_solution(15600119221481125319)
XLA Ops:
  6.5 3.2 pad_maximum_fusion
  9.7 0.0 all-gather.3.cloned.1.call-update
  9.7 0.0 copy-done.4
  9.8 0.2 select_reduce_fusion.1
  10.0 0.3 fusion.3
  10.3 3.3 convolution_convert_fusion
  13.7 11.8 %all-to-all-start = ((bf16[64,16,2048]{2,1,0:T(8,128)(2,1)}), bf16[64,16,2048]{2,1,0:T(8,128)(2,1)}, u32[]{:S(2)}, u32[]{:S(2)}) async-start(bf16[64,16,2048]{2,1,0:T(8,128)(2,1)} %bitcast.48), calls=%async_computation | async-start | bytes 8388608 | tf_op jit(solution)/shard_map/all_to_all | solution.py:46
  25.5 1.7 collective-permute-start
  27.2 47.3 %collective-permute-done = bf16[1,256,2048]{2,1,0:T(8,128)(2,1)S(1)} collective-permute-done((bf16[1,256,2048]{2,1,0:T(8,128)(2,1)S(1)}, bf16[1,256,2048]{2,1,0:T(8,128)(2,1)S(1)}, u32[]{:S(2)}, u32[]{:S(2)}) %collective-permute-start) | collective-permute-done | bytes 1048608 | tf_op jit(solution)/shard_map/ppermute | solution.py:16
  74.5 0.1 collective-permute-start.1
  74.5 48.2 %collective-permute-done.1 = bf16[1,256,2048]{2,1,0:T(8,128)(2,1)} collective-permute-done((bf16[1,256,2048]{2,1,0:T(8,128)(2,1)S(1)}, bf16[1,256,2048]{2,1,0:T(8,128)(2,1)}, u32[]{:S(2)}, u32[]{:S(2)}) %collective-permute-start.1) | collective-permute-done | bytes 1048608 | tf_op jit(solution)/shard_map/ppermute | solution.py:16
  122.8 0.0 collective-permute-start.2
  122.8 2.5 squeeze.21
  125.3 1.0 bitcast_dynamic-update-slice_fusion.3
  126.3 1.1 bitcast_dynamic-update-slice_fusion.2
  127.4 2.4 bitcast_dynamic-update-slice_fusion.1
  129.7 37.0 %collective-permute-done.2 = bf16[1,256,2048]{2,1,0:T(8,128)(2,1)} collective-permute-done((bf16[1,256,2048]{2,1,0:T(8,128)(2,1)}, bf16[1,256,2048]{2,1,0:T(8,128)(2,1)}, u32[]{:S(2)}, u32[]{:S(2)}) %collective-permute-start.2) | collective-permute-done | bytes 1048608 | tf_op jit(solution)/shard_map/ppermute | solution.py:16
  166.7 2.3 bitcast_dynamic-update-slice_fusion
  169.1 0.0 all-to-all-done
  169.1 9.9 %fusion = f32[1024,1024]{1,0:T(8,128)} fusion(bf16[1024,2048]{1,0:T(8,128)(2,1)} %bitcast.9, bf16[2,2048,1024]{2,1,0:T(8,128)(2,1)} %all-gather.3.cloned.1.call-done), kind=kOutput, calls=%fused_computation.1 | convolution fusion | flops 4294967296 | bytes 12582912 | tf_op jit(solution)/shard_map/dot_general | solution.py:51
  179.0 15.4 %convolution_convert_fusion.1 = bf16[1024,2048]{1,0:T(8,128)(2,1)} fusion(bf16[1024,2048]{1,0:T(8,128)(2,1)} %bitcast_dynamic-update-slice_fusion, f32[1024,1024]{1,0:T(8,128)} %fusion, bf16[1024,2048]{1,0:T(8,128)(2,1)} %bitcast.9, bf16[2,2048,1024]{2,1,0:T(8,128)(2,1)} %all-gather.3.cloned.1.call-done), kind=kOutput, calls=%fused_computation.6 | convolution fusion | flops 8598323200 | bytes 20971520 | tf_op jit(solution)/shard_map/dot_general | solution.py:53
  194.4 10.8 %all-to-all-start.1 = ((bf16[64,16,2048]{2,1,0:T(8,128)(2,1)}), bf16[64,16,2048]{2,1,0:T(8,128)(2,1)}, u32[]{:S(2)}, u32[]{:S(2)}) async-start(bf16[64,16,2048]{2,1,0:T(8,128)(2,1)} %bitcast.49), calls=%async_computation.1 | async-start | bytes 8388608 | tf_op jit(solution)/shard_map/all_to_all | solution.py:54
  205.3 95.2 %all-to-all-done.1 = bf16[64,16,2048]{2,1,0:T(8,128)(2,1)} async-done(((bf16[64,16,2048]{2,1,0:T(8,128)(2,1)}), bf16[64,16,2048]{2,1,0:T(8,128)(2,1)}, u32[]{:S(2)}, u32[]{:S(2)}) %all-to-all-start.1) | async-done | bytes 4194336 | tf_op jit(solution)/shard_map/all_to_all | solution.py:54
  300.4 3.6 %fusion.22 = f32[256,2048]{1,0:T(8,128)S(1)} fusion(bf16[1024,2048]{1,0:T(8,128)(2,1)} %bitcast.17, f32[256]{0:T(256)S(1)} %bitcast.59, s32[256]{0:T(256)S(1)} %bitcast.63, f32[256]{0:T(256)S(1)} %bitcast.57, s32[256]{0:T(256)S(1)} %bitcast.61), kind=kOutput, calls=%fused_computation.42 | convolution fusion | flops 1075314688 | bytes 6295552 | tf_op jit(solution)/shard_map/dot_general | solution.py:64
  304.1 3.7 %fusion.2 = bf16[256,2048]{1,0:T(8,128)(2,1)S(1)} fusion(f32[256,2048]{1,0:T(8,128)S(1)} %fusion.22, bf16[1024,2048]{1,0:T(8,128)(2,1)} %bitcast.17, bf16[256,2048]{1,0:T(8,128)(2,1)S(1)} %copy-done, f32[256]{0:T(256)S(1)} %bitcast.60, s32[256]{0:T(256)S(1)} %bitcast.64, f32[256]{0:T(256)S(1)} %bitcast.58, s32[256]{0:T(256)S(1)} %bitcast.62), kind=kOutput, calls=%fused_computation.11 | convolution fusion | flops 1078198272 | bytes 8392704 | tf_op jit(solution)/shard_map/dot_general | solution.py:64
  307.8 0.0 copy-start.5
  307.8 1.1 copy.19
  308.9 4.4 %all-to-all-start.2 = ((bf16[4,256,512]{2,1,0:T(8,128)(2,1)}), bf16[4,256,512]{2,1,0:T(8,128)(2,1)S(1)}, u32[]{:S(2)}, u32[]{:S(2)}) async-start(bf16[4,256,512]{2,1,0:T(8,128)(2,1)} %bitcast.47), calls=%async_computation.2 | async-start | bytes 2097152 | tf_op jit(solution)/shard_map/all_to_all | solution.py:69
  313.3 15.2 %all-to-all-done.2 = bf16[4,256,512]{2,1,0:T(8,128)(2,1)S(1)} async-done(((bf16[4,256,512]{2,1,0:T(8,128)(2,1)}), bf16[4,256,512]{2,1,0:T(8,128)(2,1)S(1)}, u32[]{:S(2)}, u32[]{:S(2)}) %all-to-all-start.2) | async-done | bytes 1048608 | tf_op jit(solution)/shard_map/all_to_all | solution.py:69
  328.5 0.3 multiply_reduce_fusion
  328.8 12.0 %all-gather = f32[4,1,1024]{2,1,0:T(1,128)S(1)} all-gather(f32[1,1,1024]{2,1,0:T(1,128)S(1)} %reshape.85), channel_id=1, replica_groups=mesh['ep'=64,'tp'=4] {'tp'}, dimensions={0}, use_global_device_ids=true | all-gather | bytes 20480 | tf_op jit(solution)/shard_map/all_gather | solution.py:71
  340.8 1.3 fusion.7
  (28 shorter events, 0.2 us)
Async XLA Ops:
  6.5 3.2 copy-start.4
  6.5 3.2 copy-start.3
  6.5 3.5 copy-start
  6.5 162.5 %all-gather.3.cloned.1.call-start = ((), (), s32[]{:S(2)}) async-start(), calls=%async_computation.3 | async-start | bytes 10485760 | tf_op jit(solution)/shard_map/all_gather | solution.py:28
  13.7 11.8 %copy-start.1 = (bf16[1,256,2048]{2,1,0:T(8,128)(2,1)S(1)}, bf16[1,256,2048]{2,1,0:T(8,128)(2,1)}, u32[]{:S(2)}) copy-start(bf16[1,256,2048]{2,1,0:T(8,128)(2,1)} %param.16) | copy-start | bytes 3145732
  13.7 155.4 %all-to-all-start = ((bf16[64,16,2048]{2,1,0:T(8,128)(2,1)}), bf16[64,16,2048]{2,1,0:T(8,128)(2,1)}, u32[]{:S(2)}, u32[]{:S(2)}) async-start(bf16[64,16,2048]{2,1,0:T(8,128)(2,1)} %bitcast.48), calls=%async_computation | async-start | bytes 8388608 | tf_op jit(solution)/shard_map/all_to_all | solution.py:46
  25.5 48.9 %collective-permute-start = (bf16[1,256,2048]{2,1,0:T(8,128)(2,1)S(1)}, bf16[1,256,2048]{2,1,0:T(8,128)(2,1)S(1)}, u32[]{:S(2)}, u32[]{:S(2)}) collective-permute-start(bf16[1,256,2048]{2,1,0:T(8,128)(2,1)S(1)} %copy-done.1), channel_id=1, source_target_pairs={{0,1},{1,2},{2,3},{3,0},{4,5},{5,6},{6,7},{7,4},{8,9},{9,10},{10,1... | collective-permute-start | bytes 3145736 | tf_op jit(solution)/shard_map/ppermute | solution.py:16
  74.5 48.3 %collective-permute-start.1 = (bf16[1,256,2048]{2,1,0:T(8,128)(2,1)S(1)}, bf16[1,256,2048]{2,1,0:T(8,128)(2,1)}, u32[]{:S(2)}, u32[]{:S(2)}) collective-permute-start(bf16[1,256,2048]{2,1,0:T(8,128)(2,1)S(1)} %collective-permute-done), channel_id=1, source_target_pairs={{0,1},{1,2},{2,3},{3,0},{4,5},{5,6},{6,7},{7,4},{8,9},{9,10},{10,1... | collective-permute-start | bytes 3145736 | tf_op jit(solution)/shard_map/ppermute | solution.py:16
  122.8 44.0 %collective-permute-start.2 = (bf16[1,256,2048]{2,1,0:T(8,128)(2,1)}, bf16[1,256,2048]{2,1,0:T(8,128)(2,1)}, u32[]{:S(2)}, u32[]{:S(2)}) collective-permute-start(bf16[1,256,2048]{2,1,0:T(8,128)(2,1)} %collective-permute-done.1), channel_id=1, source_target_pairs={{0,1},{1,2},{2,3},{3,0},{4,5},{5,6},{6,7},{7,4},{8,9},{9,10},{10,1... | collective-permute-start | bytes 3145736 | tf_op jit(solution)/shard_map/ppermute | solution.py:16
  194.4 10.8 %copy-start.2 = (f32[256,2]{0,1:T(2,128)S(1)}, f32[256,2]{0,1:T(2,128)}, u32[]{:S(2)}) copy-start(f32[256,2]{0,1:T(2,128)} %param.13) | copy-start | bytes 6148
  194.4 10.9 %copy-start.6 = (f32[256]{0:T(256)S(1)}, f32[256]{0:T(256)}, u32[]{:S(2)}) copy-start(f32[256]{0:T(256)} %param.12) | copy-start | bytes 3076
  194.4 106.1 %all-to-all-start.1 = ((bf16[64,16,2048]{2,1,0:T(8,128)(2,1)}), bf16[64,16,2048]{2,1,0:T(8,128)(2,1)}, u32[]{:S(2)}, u32[]{:S(2)}) async-start(bf16[64,16,2048]{2,1,0:T(8,128)(2,1)} %bitcast.49), calls=%async_computation.1 | async-start | bytes 8388608 | tf_op jit(solution)/shard_map/all_to_all | solution.py:54
  307.8 5.4 %copy-start.5 = (bf16[512]{0:T(512)(128)(2,1)S(1)}, bf16[512]{0:T(512)(128)(2,1)}, u32[]{:S(2)}) copy-start(bf16[512]{0:T(512)(128)(2,1)} %param.17) | copy-start | bytes 3076
  308.9 19.6 %all-to-all-start.2 = ((bf16[4,256,512]{2,1,0:T(8,128)(2,1)}), bf16[4,256,512]{2,1,0:T(8,128)(2,1)S(1)}, u32[]{:S(2)}, u32[]{:S(2)}) async-start(bf16[4,256,512]{2,1,0:T(8,128)(2,1)} %bitcast.47), calls=%async_computation.2 | async-start | bytes 2097152 | tf_op jit(solution)/shard_map/all_to_all | solution.py:69
Sparse Core Ops, SparseCore 0:
  9.9 155.8 all-gather.2
